TPU v7x, 128 devices: a whole 4x4x4 slice. The times are simulated.
128 devices in a mesh: rep: 2 (over z_hi), fs: 32 (over z_lo, y, x), tp: 2 (over core).
Axes of the slice: x: 4, y: 4, z: 4 (z_hi: 2, z_lo: 2; z = z_hi * 2 + z_lo), core: 2. Of those that a mesh axis runs over, the one named last changes fastest.
Arguments:
- residual: bfloat16 [32768, 2048], P(('rep', 'fs', 'tp')), may hold values from -6 to 6
- mixer_gain: float32 [2048], replicated, may hold values from 0.1 to 1.9
- gating_proj: bfloat16 [2048, 2048], P('fs', 'tp'), may hold values from -0.125 to 0.125
- spatial_proj: bfloat16 [2048, 2048], P('fs', 'tp'), as said below
- spatial_gain: float32 [2048], replicated, may hold values from 0.1 to 1.9
- spatial_bias: float32 [2048], replicated, may hold values from -3 to 3
- spatial_mix: bfloat16 [32, 128, 128], replicated, may hold values from -0.5 to 0.5
- spatial_offset: float32 [32, 128], replicated, may hold values from 0.5 to 1.5
- mixer_out: bfloat16 [2048, 2048], P('tp', 'fs'), may hold values from -0.125 to 0.125
- channel_gain: float32 [2048], replicated, may hold values from 0.1 to 1.9
- gate_proj: bfloat16 [2048, 2816], P('fs', 'tp'), may hold values from -0.125 to 0.125
- up_proj: bfloat16 [2048, 2816], P('fs', 'tp'), may hold values from -0.125 to 0.125
- conv_taps: float32 [3, 2816], replicated, may hold values from -3.5 to 3.5
- down_proj: bfloat16 [2816, 2048], P('tp', 'fs'), may hold values from -0.109375 to 0.109375
Outputs:
- layer_out: bfloat16 [32768, 2048], P(('rep', 'fs', 'tp'))
Inputs may be any that keep to these rules, and one draw needn't show every extreme that they name: `spatial_proj`: entries are bounded in magnitude by 56 / sqrt(2048).
All inputs are finite; a program needn't handle non-finite values.
Results may differ from a plain program's by a relative error of at most 0.015.
Values may be sent and summed in bfloat16 or wider, within the bound.
No kernel may reach another device: no remote copies, remote signals or barrier semaphores. Data moves between devices by JAX's collectives and lax.ppermute only.
A program may use at most 128 MiB of HBM per device.

v0:
```python
import jax
import jax.numpy as jnp
from jax import lax
from jax.sharding import Mesh
from jax.sharding import PartitionSpec as P

HEAD = 64
GROUP = 2048
BLOCK = 128
SEGMENT = 64
KCONV = 3
SEQ_LEN = 256
FS = ("fs_0", "fs_1", "fs_2")
REP_FS_TP = ("rep", "fs_0", "fs_1", "fs_2", "tp")


def in_order(pieces, dim):
    pieces = jnp.moveaxis(pieces, 0, dim)
    lengths = pieces.shape
    return pieces.reshape(*lengths[:dim], lengths[dim] * lengths[dim + 1], *lengths[dim + 2 :])


def copy_for_each(value, axis):
    devices = lax.axis_size(axis)
    return lax.all_to_all(
        jnp.broadcast_to(value[None], (devices, *value.shape)), axis, 0, 0, tiled=True
    )


def gathered_copies(value, axis, dim):
    return in_order(copy_for_each(value, axis), dim)


def side_by_side(arrays, axis, dim, along):
    widths = [a.shape[along] for a in arrays]
    both = jnp.concatenate(arrays, axis=along)
    out = lax.all_gather(both, axis, axis=dim, tiled=True)
    return tuple(jnp.split(out, [sum(widths[:k]) for k in range(1, len(widths))], axis=along))


def of_everyone(value, axis):
    return copy_for_each(value, axis).sum(axis=0)


def in_one(arrays, axis):
    ends = [0]
    for a in arrays:
        ends.append(ends[-1] + a.size)
    running = of_everyone(jnp.concatenate([a.ravel() for a in arrays]), axis)
    return tuple((running[b:e].reshape(a.shape) for a, b, e in zip(arrays, ends, ends[1:])))


def stacked_from(value, axes, order):
    pieces = value[None]
    for k in order:
        pieces = lax.all_gather(pieces, axes[k], axis=0, tiled=True)
    block = [lax.axis_size(axes[k]) for k in reversed(order)]
    pieces = pieces.reshape(*block, *value.shape)
    turned = sorted(range(len(order)), key=lambda place: order[len(order) - 1 - place])
    return pieces.transpose(*turned, *range(len(order), pieces.ndim)).reshape(-1, *value.shape)


def gather_axes(value, axes, order, dim):
    return in_order(stacked_from(value, axes, order), dim)


def cut_along(value, dim, devices):
    before, after = (value.shape[:dim], value.shape[dim + 1 :])
    return jnp.moveaxis(value.reshape(*before, devices, -1, *after), dim, 0)


def sum_at_owner(value, axis, dim):
    pieces = cut_along(value, dim, lax.axis_size(axis))
    arrived = lax.all_to_all(pieces, axis, split_axis=0, concat_axis=0, tiled=True)
    return arrived.astype(jnp.float32).sum(axis=0)


def round_trip(value):
    return lax.optimization_barrier(value.astype(jnp.bfloat16)).astype(jnp.float32)


def rms_normed(value, gain):
    wide = value.astype(jnp.float32)
    scale = lax.rsqrt(jnp.mean(wide * wide, axis=-1, keepdims=True) + 1e-06)
    return (wide * scale * gain).astype(jnp.bfloat16)


def fold_pair(normed, pieces):
    first = jnp.dot(normed, pieces[0], preferred_element_type=jnp.float32)
    second = jnp.dot(normed, pieces[1], preferred_element_type=jnp.float32)
    return (first, second)


def on_device(
    residual,
    mixer_gain,
    gating_proj,
    spatial_proj,
    spatial_gain,
    spatial_bias,
    spatial_mix,
    spatial_offset,
    mixer_out,
    channel_gain,
    gate_proj,
    up_proj,
    conv_taps,
    down_proj,
):
    position = lax.axis_index("tp")
    rows = gathered_copies(residual, "tp", 0)
    group_rows = rows.shape[0]
    normed = rms_normed(rows, mixer_gain)
    width = gating_proj.shape[1]
    gating, spatial = fold_pair(normed, side_by_side((gating_proj, spatial_proj), FS, 0, 1))
    act_u = jax.nn.gelu(round_trip(gating))
    act_v = jax.nn.gelu(round_trip(spatial))
    total, squares = in_one((jnp.sum(act_v, axis=-1), jnp.sum(act_v * act_v, axis=-1)), "tp")
    mean = (total / GROUP)[:, None]
    var = (squares / GROUP)[:, None] - mean * mean
    gain_here = lax.dynamic_slice_in_dim(spatial_gain, position * width, width)
    bias_here = lax.dynamic_slice_in_dim(spatial_bias, position * width, width)
    vnorm = ((act_v - mean) * lax.rsqrt(var + 1e-05) * gain_here + bias_here).astype(jnp.bfloat16)
    heads_here = width // HEAD
    mix_here = lax.dynamic_slice_in_dim(spatial_mix, position * heads_here, heads_here, 0)
    offset_here = lax.dynamic_slice_in_dim(spatial_offset, position * heads_here, heads_here, 0)
    place = jnp.arange(BLOCK) // SEGMENT
    allowed = place[None, :] <= place[:, None]
    weights = jnp.where(allowed[None], mix_here, jnp.zeros_like(mix_here))
    blocks = vnorm.reshape(group_rows // BLOCK, BLOCK, heads_here, HEAD)
    mixed = jnp.einsum("hij,njhd->nihd", weights, blocks, preferred_element_type=jnp.float32)
    mixed = mixed + offset_here.T[None, :, :, None]
    gated = (act_u * mixed.reshape(group_rows, width)).astype(jnp.bfloat16)
    out_whole = gather_axes(mixer_out, FS, (0, 1, 2), 1)
    part = gated
    mixer_part = sum_at_owner(
        jnp.dot(part, out_whole, preferred_element_type=jnp.float32).astype(jnp.bfloat16), "tp", 0
    )
    middle = (residual.astype(jnp.float32) + mixer_part).astype(jnp.bfloat16)
    rows2 = gathered_copies(middle, "tp", 0)
    normed2 = rms_normed(rows2, channel_gain)
    units = gate_proj.shape[1]
    gate_whole, up_whole = side_by_side((gate_proj, up_proj), FS, 0, 1)
    gate = jnp.dot(normed2, gate_whole, preferred_element_type=jnp.float32)
    up = jnp.dot(normed2, up_whole, preferred_element_type=jnp.float32)
    gate = round_trip(gate)
    up = round_trip(up)
    taps_here = lax.dynamic_slice_in_dim(conv_taps, position * units, units, 1)
    offset = jnp.arange(group_rows) % SEQ_LEN
    conv = taps_here[KCONV - 1] * gate
    for lag in range(1, KCONV):
        shifted = jnp.concatenate([jnp.zeros((lag, units), jnp.float32), gate[:-lag]], axis=0)
        shifted = jnp.where((offset >= lag)[:, None], shifted, 0.0)
        conv = conv + taps_here[KCONV - 1 - lag] * shifted
    hidden = (jax.nn.silu(conv) * up).astype(jnp.bfloat16)
    down_whole = lax.all_gather(down_proj, FS, axis=1, tiled=True)
    part = hidden
    channel_part = sum_at_owner(
        jnp.dot(part, down_whole, preferred_element_type=jnp.float32).astype(jnp.bfloat16), "tp", 0
    )
    return (middle.astype(jnp.float32) + channel_part).astype(jnp.bfloat16)


def solution(mesh):
    split = Mesh(
        mesh.devices.reshape(mesh.shape["rep"], 2, 4, 4, mesh.shape["tp"]),
        ("rep", "fs_0", "fs_1", "fs_2", "tp"),
    )
    placed = (
        P(REP_FS_TP, None),
        P(),
        P(FS, "tp"),
        P(FS, "tp"),
        P(),
        P(),
        P(),
        P(),
        P("tp", FS),
        P(),
        P(FS, "tp"),
        P(FS, "tp"),
        P(),
        P("tp", FS),
    )
    return jax.shard_map(
        on_device, mesh=split, in_specs=placed, out_specs=P(REP_FS_TP, None), check_vma=False
    )
```

profile of v0, /device:TPU:1, one launch (start us, length us, event | category | flops | bytes accessed | tf_op | source)
XLA Modules:
  0.0 617.4 jit_solution(9370628572742280357)
XLA Ops:
  6.6 6.7 %all-gather = bf16[2048,64]{0,1:T(8,128)(2,1)S(1)} all-gather(bf16[1024,64]{0,1:T(8,128)(2,1)} %param.22), channel_id=2, replica_groups=mesh['rep'=2,'fs_0'=2,'fs_1'=4,'fs_2'=4,'tp'=2] {'fs_0'}, dimensions={0}, use_global_device_ids=true | all-gather | bytes 393216 | tf_op jit(solution)/shard_map/all_gather | solution.py:56
  14.1 24.9 %all-gather.9.cloned.1.call-done = bf16[8,1024,64]{1,2,0:T(8,128)(2,1)} async-done(((bf16[2,1024,64]{1,2,0:T(8,128)(2,1)}), bf16[8,1024,64]{1,2,0:T(8,128)(2,1)}) %all-gather.9.cloned.1.call-update) | async-done | bytes 1048592 | tf_op jit(solution)/shard_map/all_gather | solution.py:56
  41.3 1.6 broadcast_in_dim.32
  42.9 6.5 %all-to-all-start = ((bf16[2,256,2048]{2,1,0:T(8,128)(2,1)}), bf16[2,256,2048]{2,1,0:T(8,128)(2,1)S(1)}, u32[]{:S(2)}, u32[]{:S(2)}) async-start(bf16[2,256,2048]{2,1,0:T(8,128)(2,1)} %broadcast_in_dim.32), calls=%async_computation | async-start | bytes 4194304 | tf_op jit(solution)/shard_map/all_to_all | solution.py:25
  49.4 2.5 all-to-all-done
  52.4 1.6 dynamic-slice_reduce_fusion.2
  54.7 1.9 fusion.11
  56.5 34.6 %all-gather.11.cloned.1.call-done = bf16[32,1024,64]{1,2,0:T(8,128)(2,1)} async-done(((bf16[8,1024,64]{1,2,0:T(8,128)(2,1)}), bf16[32,1024,64]{1,2,0:T(8,128)(2,1)}) %all-gather.11.cloned.1.call-update) | async-done | bytes 4194320 | tf_op jit(solution)/shard_map/all_gather | solution.py:56
  91.1 4.9 copy.56
  96.0 143.2 %all-gather.7.cloned.1.call-done = bf16[2048,2048]{1,0:T(8,128)(2,1)} async-done(((bf16[64,2048]{1,0:T(8,128)(2,1)}), bf16[2048,2048]{1,0:T(8,128)(2,1)}) %all-gather.7.cloned.1.call-update) | async-done | bytes 8388624 | tf_op jit(solution)/shard_map/all_gather | solution.py:37
  239.2 5.1 fusion.37
  245.3 24.3 %all_to_all.26 = f32[2,1,1024]{2,1,0:T(1,128)S(1)} all-to-all(f32[2,1,1024]{2,1,0:T(1,128)S(1)} %broadcast_in_dim.33), channel_id=1, replica_groups=mesh['rep'=2,'fs_0'=2,'fs_1'=4,'fs_2'=4,'tp'=2] {'tp'}, dimensions={0} | all-to-all | bytes 16384 | tf_op jit(solution)/shard_map/all_to_all | solution.py:25
  269.7 1.0 add_convert_fusion.2
  270.7 2.3 reshape.157
  273.1 2.7 bitcast_add_fusion
  275.8 3.0 copy.60
  278.8 3.5 reshape.158
  282.3 5.4 fusion.34
  287.7 2.7 convolution_convert_fusion
  290.4 5.3 all_to_all.27
  296.8 5.5 all_to_all.28
  303.0 1.9 fusion.9
  304.9 109.0 %all-gather.13.cloned.1.call-done = bf16[2048,2816]{1,0:T(8,128)(2,1)} async-done(((bf16[64,2816]{1,0:T(8,128)(2,1)}), bf16[2048,2816]{1,0:T(8,128)(2,1)}) %all-gather.13.cloned.1.call-update) | async-done | bytes 11534352 | tf_op jit(solution)/shard_map/all_gather | solution.py:37
  413.9 6.8 %fusion.12 = bf16[512,1408]{1,0:T(8,128)(2,1)S(1)} fusion(bf16[512,2048]{1,0:T(8,128)(2,1)} %fusion.9, bf16[2048,2816]{1,0:T(8,128)(2,1)} %all-gather.13.cloned.1.call-done), kind=kOutput, calls=%fused_computation.27 | convolution fusion | flops 2953510912 | bytes 9306112 | tf_op jit(solution)/shard_map/dot_general | solution.py:144
  420.7 1.7 slice.28
  422.4 1.9 slice.29
  424.3 1.2 copy-done.4
  425.5 4.5 fusion.15
  430.0 144.2 %all-gather.15.cloned.1.call-done = bf16[1408,2048]{0,1:T(8,128)(2,1)} async-done(((bf16[1408,64]{0,1:T(8,128)(2,1)}), bf16[1408,2048]{0,1:T(8,128)(2,1)}) %all-gather.15.cloned.1.call-update) | async-done | bytes 5767184 | tf_op jit(solution)/shard_map/all_gather | solution.py:156
  574.2 9.8 %convolution_convert_fusion.1 = bf16[512,2048]{1,0:T(8,128)(2,1)S(1)} fusion(bf16[1408,2048]{0,1:T(8,128)(2,1)} %all-gather.15.cloned.1.call-done, bf16[512,1408]{1,0:T(8,128)(2,1)} %fusion.15, f32[510,1408]{1,0:T(8,128)} %slice.29, f32[511,1408]{1,0:T(8,128)} %slice.28, f32[1408]{0:T(1024)S(1)} %copy-done.13, f32[1408]{0:T(1024)S(1)} %copy-done.12, ...), kind=kOutput, calls=%fused_computation.29 | convolution fusion | flops 2964652032 | bytes 16516096 | tf_op jit(solution)/shard_map/dot_general | solution.py:159
  584.0 25.1 %all_to_all.29 = bf16[2,256,2048]{2,1,0:T(8,128)(2,1)S(1)} all-to-all(bf16[2,256,2048]{2,1,0:T(8,128)(2,1)S(1)} %bitcast.51), channel_id=1, replica_groups=mesh['rep'=2,'fs_0'=2,'fs_1'=4,'fs_2'=4,'tp'=2] {'tp'}, dimensions={0} | all-to-all | bytes 4194304 | tf_op jit(solution)/shard_map/all_to_all | solution.py:74
  609.6 1.3 add_convert_fusion
  (74 shorter events, 7.5 us)
Async XLA Ops:
  6.5 48.0 %copy-start = (f32[32,128]{1,0:T(8,128)S(1)}, f32[32,128]{1,0:T(8,128)}, u32[]{:S(2)}) copy-start(f32[32,128]{1,0:T(8,128)} %param.21) | copy-start | bytes 49156
  6.5 32.5 %copy-start.8 = (bf16[64,1024]{1,0:T(8,128)(2,1)S(1)}, bf16[64,1024]{1,0:T(8,128)(2,1)}, u32[]{:S(2)}) copy-start(bf16[64,1024]{1,0:T(8,128)(2,1)} %param.16) | copy-start | bytes 393220
  6.5 32.5 %copy-start.7 = (bf16[64,1024]{1,0:T(8,128)(2,1)S(1)}, bf16[64,1024]{1,0:T(8,128)(2,1)}, u32[]{:S(2)}) copy-start(bf16[64,1024]{1,0:T(8,128)(2,1)} %param.17) | copy-start | bytes 393220
  6.5 33.3 %copy-start.6 = (bf16[64,1408]{1,0:T(8,128)(2,1)S(1)}, bf16[64,1408]{1,0:T(8,128)(2,1)}, u32[]{:S(2)}) copy-start(bf16[64,1408]{1,0:T(8,128)(2,1)} %param.24) | copy-start | bytes 540676
  6.5 33.3 %copy-start.5 = (bf16[64,1408]{1,0:T(8,128)(2,1)S(1)}, bf16[64,1408]{1,0:T(8,128)(2,1)}, u32[]{:S(2)}) copy-start(bf16[64,1408]{1,0:T(8,128)(2,1)} %param.25) | copy-start | bytes 540676
  6.5 34.7 %copy-start.3 = (bf16[256,2048]{1,0:T(8,128)(2,1)S(1)}, bf16[256,2048]{1,0:T(8,128)(2,1)}, u32[]{:S(2)}) copy-start(bf16[256,2048]{1,0:T(8,128)(2,1)} %param.14) | copy-start | bytes 3145732
  6.6 32.4 %all-gather.9.cloned.1.call-start = ((), (), s32[]{:S(2)}) async-start(), calls=%async_computation.6 | async-start | bytes 1310720 | tf_op jit(solution)/shard_map/all_gather | solution.py:56
  14.1 77.0 %all-gather.11.cloned.1.call-start = ((), (), s32[]{:S(2)}) async-start(), calls=%async_computation.7 | async-start | bytes 5242880 | tf_op jit(solution)/shard_map/all_gather | solution.py:56
  39.0 200.2 %all-gather.7.cloned.1.call-start = ((), (), s32[]{:S(2)}) async-start(), calls=%async_computation.5 | async-start | bytes 8650752 | tf_op jit(solution)/shard_map/all_gather | solution.py:37
  39.8 374.0 %all-gather.13.cloned.1.call-start = ((), (), s32[]{:S(2)}) async-start(), calls=%async_computation.8 | async-start | bytes 11894784 | tf_op jit(solution)/shard_map/all_gather | solution.py:37
  40.7 533.5 %all-gather.15.cloned.1.call-start = ((), (), s32[]{:S(2)}) async-start(), calls=%async_computation.9 | async-start | bytes 5947392 | tf_op jit(solution)/shard_map/all_gather | solution.py:156
  42.9 9.0 %all-to-all-start = ((bf16[2,256,2048]{2,1,0:T(8,128)(2,1)}), bf16[2,256,2048]{2,1,0:T(8,128)(2,1)S(1)}, u32[]{:S(2)}, u32[]{:S(2)}) async-start(bf16[2,256,2048]{2,1,0:T(8,128)(2,1)} %broadcast_in_dim.32), calls=%async_computation | async-start | bytes 4194304 | tf_op jit(solution)/shard_map/all_to_all | solution.py:25
  49.4 5.3 copy-start.9
  96.0 173.8 %dynamic-slice-start = ((f32[2048]{0:T(1024)}, s32[]{:T(128)}), f32[1024]{0:T(1024)S(1)}, s32[]{:S(2)}) async-start(f32[2048]{0:T(1024)} %param.18, s32[]{:T(128)} %select_n.51), calls=%async_computation.10 | async-start | bytes 8704 | tf_op jit(solution)/shard_map/dynamic_slice | solution.py:121
  96.0 173.8 %dynamic-slice-start.1 = ((f32[2048]{0:T(1024)}, s32[]{:T(128)}), f32[1024]{0:T(1024)S(1)}, s32[]{:S(2)}) async-start(f32[2048]{0:T(1024)} %param.19, s32[]{:T(128)} %select_n.51), calls=%async_computation.11 | async-start | bytes 8704 | tf_op jit(solution)/shard_map/dynamic_slice | solution.py:122
  282.3 5.4 copy-start.2
  302.3 0.7 copy-start.10
  413.9 10.4 %slice-start = ((s8[11534336]{0:T(1024)(128)(4,1)}), s8[4194304]{0:T(1024)(128)(4,1)S(1)}, s32[]{:S(2)}) async-start(s8[11534336]{0:T(1024)(128)(4,1)} %bitcast.57), calls=%async_computation.12 | async-start | bytes 8388608
  413.9 10.4 %slice-start.1 = ((s8[11534336]{0:T(1024)(128)(4,1)}), s8[4194304]{0:T(1024)(128)(4,1)S(1)}, s32[]{:S(2)}) async-start(s8[11534336]{0:T(1024)(128)(4,1)} %bitcast.57), calls=%async_computation.13 | async-start | bytes 8388608
  420.7 3.6 slice-start.2
  422.4 3.1 copy-start.4
  425.5 148.7 %copy-start.11 = (f32[1408]{0:T(1024)S(1)}, f32[1408]{0:T(1024)}, u32[]{:S(2)}) copy-start(f32[1408]{0:T(1024)} %get-tuple-element.7) | copy-start | bytes 16900
  425.5 148.7 %copy-start.12 = (f32[1408]{0:T(1024)S(1)}, f32[1408]{0:T(1024)}, u32[]{:S(2)}) copy-start(f32[1408]{0:T(1024)} %get-tuple-element.8) | copy-start | bytes 16900
  425.5 148.7 %copy-start.13 = (f32[1408]{0:T(1024)S(1)}, f32[1408]{0:T(1024)}, u32[]{:S(2)}) copy-start(f32[1408]{0:T(1024)} %get-tuple-element.9) | copy-start | bytes 16900
  425.5 148.7 %copy-start.14 = (pred[512]{0:T(512)(128)(4,1)S(1)}, pred[512]{0:T(512)(128)(4,1)}, u32[]{:S(2)}) copy-start(pred[512]{0:T(512)(128)(4,1)} %get-tuple-element.12) | copy-start | bytes 1540
  425.5 148.7 %copy-start.15 = (pred[512]{0:T(512)(128)(4,1)S(1)}, pred[512]{0:T(512)(128)(4,1)}, u32[]{:S(2)}) copy-start(pred[512]{0:T(512)(128)(4,1)} %get-tuple-element.13) | copy-start | bytes 1540
  609.1 1.8 copy-start.1
Sparse Core Ops, SparseCore 0:
  14.2 24.7 all-gather.8
  40.6 50.3 all-gather.10
  92.7 146.3 all-gather.6
  240.7 173.1 all-gather.12
  415.4 158.7 all-gather.14
where the time goes:
time: 618 us; the launch traced here: 617 us
  waiting for transfers between devices  459 us (74%)
  blocking collectives  67.1 us (11%)
  matrix products  37 us (6%)
  local copies, waits for them, and re-layouts  22.9 us (4%)
  between operations  13.4 us (2%)
  other arithmetic  11.5 us (2%)
  starting transfers between devices  6.7 us (1%)
    all_gather x2, waiting for transfers between devices, side_by_side(): out = lax.all_gather(both, axis, axis=dim, tiled=True)  252 us
    all_gather x1, waiting for transfers between devices, on_device(): down_whole = lax.all_gather(down_proj, FS, axis=1, tiled=True)  144 us
    all_gather x2, waiting for transfers between devices, stacked_from(): pieces = lax.all_gather(pieces, axes[k], axis=0, tiled=True)  59.4 us
    all_to_all x2, blocking collectives, sum_at_owner(): lax.all_to_all(pieces, axis, split_axis=0, concat_axis=0, tiled=True)  30.5 us
    all_to_all x2, blocking collectives, copy_for_each(): lax.all_to_all(jnp.broadcast_to(value[None], (devices, *value.shape)), ax...  29.9 us
  transfers between devices with their start and end apart: 6, of which 6 were waited for; matrix products, arithmetic and copies ran while one was open for 9% of the time, Pallas kernels for 0%

commit v1 on v0

--- a/solution.py
+++ b/solution.py
@@ -153,7 +153,10 @@
         shifted = jnp.where((offset >= lag)[:, None], shifted, 0.0)
         conv = conv + taps_here[KCONV - 1 - lag] * shifted
     hidden = (jax.nn.silu(conv) * up).astype(jnp.bfloat16)
-    down_whole = lax.all_gather(down_proj, FS, axis=1, tiled=True)
+    size = lax.axis_size(FS)
+    tiles = jnp.stack([down_proj for _ in range(size)])
+    tiles = lax.all_to_all(tiles, FS, split_axis=0, concat_axis=0)
+    down_whole = jnp.concatenate(tiles, axis=1)
     part = hidden
     channel_part = sum_at_owner(
         jnp.dot(part, down_whole, preferred_element_type=jnp.float32).astype(jnp.bfloat16), "tp", 0

time: 618 us -> 537 us (0.87)
  waiting for transfers between devices: 459 us -> 374 us
  starting transfers between devices: 6.7 us -> 14 us
    all_gather x1 -> x0, waiting for transfers between devices: 144 us -> none  [on_device(): down_whole = lax.all_gather(down_proj, FS, axis=1, tiled=True)]
    all_gather x2, waiting for transfers between devices: 252 us -> 309 us  [side_by_side(): out = lax.all_gather(both, axis, axis=dim, tiled=True)]
    all_to_all x0 -> x1, starting transfers between devices: none -> 7.37 us  [on_device(): tiles = lax.all_to_all(tiles, FS, split_axis=0, concat_axis=0)]
  transfers between devices with their start and end apart: 6 -> 6, of which waited for: 6 -> 5; matrix products, arithmetic and copies ran while one was open for 9% -> 11% of each run, Pallas kernels for 0% -> 0%
where the time goes in v1:
time: 537 us
  waiting for transfers between devices  374 us (70%)
  blocking collectives  62.1 us (12%)
  matrix products  37 us (7%)
  local copies, waits for them, and re-layouts  25.4 us (5%)
  starting transfers between devices  14 us (3%)
  between operations  13.4 us (2%)
  other arithmetic  11 us (2%)
    all_gather x2, waiting for transfers between devices, side_by_side(): out = lax.all_gather(both, axis, axis=dim, tiled=True)  309 us
    all_gather x2, waiting for transfers between devices, stacked_from(): pieces = lax.all_gather(pieces, axes[k], axis=0, tiled=True)  62 us
    all_to_all x2, blocking collectives, copy_for_each(): lax.all_to_all(jnp.broadcast_to(value[None], (devices, *value.shape)), ax...  29.9 us
    all_to_all x2, blocking collectives, sum_at_owner(): lax.all_to_all(pieces, axis, split_axis=0, concat_axis=0, tiled=True)  25.5 us
  transfers between devices with their start and end apart: 6, of which 5 were waited for; matrix products, arithmetic and copies ran while one was open for 11% of the time, Pallas kernels for 0%

profile of v1, /device:TPU:1, one launch (start us, length us, event | category | flops | bytes accessed | tf_op | source)
XLA Modules:
  0.0 536.7 jit_solution(10030381703385342435)
XLA Ops:
  6.6 6.7 %all-gather = bf16[2048,64]{0,1:T(8,128)(2,1)S(1)} all-gather(bf16[1024,64]{0,1:T(8,128)(2,1)} %param.22), channel_id=2, replica_groups=mesh['rep'=2,'fs_0'=2,'fs_1'=4,'fs_2'=4,'tp'=2] {'fs_0'}, dimensions={0}, use_global_device_ids=true | all-gather | bytes 393216 | tf_op jit(solution)/shard_map/all_gather | solution.py:56
  14.1 24.9 %all-gather.8.cloned.1.call-done = bf16[8,1024,64]{1,2,0:T(8,128)(2,1)} async-done(((bf16[2,1024,64]{1,2,0:T(8,128)(2,1)}), bf16[8,1024,64]{1,2,0:T(8,128)(2,1)}) %all-gather.8.cloned.1.call-update) | async-done | bytes 1048592 | tf_op jit(solution)/shard_map/all_gather | solution.py:56
  40.7 1.6 broadcast_in_dim.32
  42.3 6.5 %all-to-all-start = ((bf16[2,256,2048]{2,1,0:T(8,128)(2,1)}), bf16[2,256,2048]{2,1,0:T(8,128)(2,1)S(1)}, u32[]{:S(2)}, u32[]{:S(2)}) async-start(bf16[2,256,2048]{2,1,0:T(8,128)(2,1)} %broadcast_in_dim.32), calls=%async_computation | async-start | bytes 4194304 | tf_op jit(solution)/shard_map/all_to_all | solution.py:25
  48.8 2.5 all-to-all-done
  52.0 2.0 fusion.11
  54.0 37.1 %all-gather.10.cloned.1.call-done = bf16[32,1024,64]{1,2,0:T(8,128)(2,1)} async-done(((bf16[8,1024,64]{1,2,0:T(8,128)(2,1)}), bf16[32,1024,64]{1,2,0:T(8,128)(2,1)}) %all-gather.10.cloned.1.call-update) | async-done | bytes 4194320 | tf_op jit(solution)/shard_map/all_gather | solution.py:56
  91.1 5.0 copy.57
  96.1 143.1 %all-gather.6.cloned.1.call-done = bf16[2048,2048]{1,0:T(8,128)(2,1)} async-done(((bf16[64,2048]{1,0:T(8,128)(2,1)}), bf16[2048,2048]{1,0:T(8,128)(2,1)}) %all-gather.6.cloned.1.call-update) | async-done | bytes 8388624 | tf_op jit(solution)/shard_map/all_gather | solution.py:37
  239.2 5.2 fusion.37
  245.3 24.3 %all_to_all.31 = f32[2,1,1024]{2,1,0:T(1,128)S(1)} all-to-all(f32[2,1,1024]{2,1,0:T(1,128)S(1)} %broadcast_in_dim.33), channel_id=1, replica_groups=mesh['rep'=2,'fs_0'=2,'fs_1'=4,'fs_2'=4,'tp'=2] {'tp'}, dimensions={0} | all-to-all | bytes 16384 | tf_op jit(solution)/shard_map/all_to_all | solution.py:25
  269.7 1.0 add_convert_fusion.2
  270.8 2.3 reshape.167
  273.1 2.7 bitcast_add_fusion
  275.8 3.0 copy.61
  278.8 3.5 reshape.168
  282.3 5.4 fusion.34
  287.7 2.7 convolution_convert_fusion
  290.4 5.4 all_to_all.32
  296.8 5.5 %all_to_all.33 = bf16[2,256,2048]{2,1,0:T(8,128)(2,1)S(1)} all-to-all(bf16[2,256,2048]{2,1,0:T(8,128)(2,1)S(1)} %broadcast_in_dim.37), channel_id=1, replica_groups=mesh['rep'=2,'fs_0'=2,'fs_1'=4,'fs_2'=4,'tp'=2] {'tp'}, dimensions={0} | all-to-all | bytes 4194304 | tf_op jit(solution)/shard_map/all_to_all | solution.py:25
  302.3 3.2 stack.2
  305.5 7.4 %all-to-all-start.4 = ((bf16[32,1408,64]{1,2,0:T(8,128)(2,1)}), bf16[32,1408,64]{1,2,0:T(8,128)(2,1)}, u32[]{:S(2)}, u32[]{:S(2)}) async-start(bf16[32,1408,64]{1,2,0:T(8,128)(2,1)} %stack.2), calls=%async_computation.4 | async-start | bytes 11534336 | tf_op jit(solution)/shard_map/all_to_all | solution.py:158
  314.4 1.9 fusion.9
  316.3 166.0 %all-gather.12.cloned.1.call-done = bf16[2048,2816]{1,0:T(8,128)(2,1)} async-done(((bf16[64,2816]{1,0:T(8,128)(2,1)}), bf16[2048,2816]{1,0:T(8,128)(2,1)}) %all-gather.12.cloned.1.call-update) | async-done | bytes 11534352 | tf_op jit(solution)/shard_map/all_gather | solution.py:37
  482.3 6.8 %fusion.12 = bf16[512,1408]{1,0:T(8,128)(2,1)S(1)} fusion(bf16[512,2048]{1,0:T(8,128)(2,1)} %fusion.9, bf16[2048,2816]{1,0:T(8,128)(2,1)} %all-gather.12.cloned.1.call-done), kind=kOutput, calls=%fused_computation.27 | convolution fusion | flops 2953510912 | bytes 9306112 | tf_op jit(solution)/shard_map/dot_general | solution.py:144
  489.1 1.7 slice.28
  490.9 1.8 slice.29
  492.7 1.2 copy-done.4
  493.9 4.5 fusion.15
  498.4 9.8 %convolution_convert_fusion.1 = bf16[512,2048]{1,0:T(8,128)(2,1)S(1)} fusion(bf16[1408,2048]{0,1:T(8,128)(2,1)} %bitcast.13, bf16[512,1408]{1,0:T(8,128)(2,1)} %fusion.15, f32[510,1408]{1,0:T(8,128)} %slice.29, f32[511,1408]{1,0:T(8,128)} %slice.28, f32[1408]{0:T(1024)S(1)} %get-tuple-element.9, f32[1408]{0:T(1024)S(1)} %get-tuple-element.8, ...), kind=kOutput, calls=%fused_computation.29 | convolution fusion | flops 2964652032 | bytes 16516096 | tf_op jit(solution)/shard_map/dot_general | solution.py:162
  508.2 20.2 %all_to_all.34 = bf16[2,256,2048]{2,1,0:T(8,128)(2,1)S(1)} all-to-all(bf16[2,256,2048]{2,1,0:T(8,128)(2,1)S(1)} %bitcast.54), channel_id=1, replica_groups=mesh['rep'=2,'fs_0'=2,'fs_1'=4,'fs_2'=4,'tp'=2] {'tp'}, dimensions={0} | all-to-all | bytes 4194304 | tf_op jit(solution)/shard_map/all_to_all | solution.py:74
  528.8 1.3 add_convert_fusion
  (66 shorter events, 7.0 us)
Async XLA Ops:
  6.5 45.3 %copy-start = (f32[32,128]{1,0:T(8,128)S(1)}, f32[32,128]{1,0:T(8,128)}, u32[]{:S(2)}) copy-start(f32[32,128]{1,0:T(8,128)} %param.21) | copy-start | bytes 49156
  6.5 32.5 %copy-start.9 = (bf16[64,1024]{1,0:T(8,128)(2,1)S(1)}, bf16[64,1024]{1,0:T(8,128)(2,1)}, u32[]{:S(2)}) copy-start(bf16[64,1024]{1,0:T(8,128)(2,1)} %param.16) | copy-start | bytes 393220
  6.5 32.5 %copy-start.8 = (bf16[64,1024]{1,0:T(8,128)(2,1)S(1)}, bf16[64,1024]{1,0:T(8,128)(2,1)}, u32[]{:S(2)}) copy-start(bf16[64,1024]{1,0:T(8,128)(2,1)} %param.17) | copy-start | bytes 393220
  6.5 33.3 %copy-start.7 = (bf16[64,1408]{1,0:T(8,128)(2,1)S(1)}, bf16[64,1408]{1,0:T(8,128)(2,1)}, u32[]{:S(2)}) copy-start(bf16[64,1408]{1,0:T(8,128)(2,1)} %param.24) | copy-start | bytes 540676
  6.5 33.3 %copy-start.6 = (bf16[64,1408]{1,0:T(8,128)(2,1)S(1)}, bf16[64,1408]{1,0:T(8,128)(2,1)}, u32[]{:S(2)}) copy-start(bf16[64,1408]{1,0:T(8,128)(2,1)} %param.25) | copy-start | bytes 540676
  6.5 34.1 %copy-start.3 = (bf16[256,2048]{1,0:T(8,128)(2,1)S(1)}, bf16[256,2048]{1,0:T(8,128)(2,1)}, u32[]{:S(2)}) copy-start(bf16[256,2048]{1,0:T(8,128)(2,1)} %param.14) | copy-start | bytes 3145732
  6.6 32.4 %all-gather.8.cloned.1.call-start = ((), (), s32[]{:S(2)}) async-start(), calls=%async_computation.7 | async-start | bytes 1310720 | tf_op jit(solution)/shard_map/all_gather | solution.py:56
  14.1 77.0 %all-gather.10.cloned.1.call-start = ((), (), s32[]{:S(2)}) async-start(), calls=%async_computation.8 | async-start | bytes 5242880 | tf_op jit(solution)/shard_map/all_gather | solution.py:56
  39.0 200.2 %all-gather.6.cloned.1.call-start = ((), (), s32[]{:S(2)}) async-start(), calls=%async_computation.6 | async-start | bytes 8650752 | tf_op jit(solution)/shard_map/all_gather | solution.py:37
  39.8 442.5 %all-gather.12.cloned.1.call-start = ((), (), s32[]{:S(2)}) async-start(), calls=%async_computation.9 | async-start | bytes 11894784 | tf_op jit(solution)/shard_map/all_gather | solution.py:37
  42.3 9.0 %all-to-all-start = ((bf16[2,256,2048]{2,1,0:T(8,128)(2,1)}), bf16[2,256,2048]{2,1,0:T(8,128)(2,1)S(1)}, u32[]{:S(2)}, u32[]{:S(2)}) async-start(bf16[2,256,2048]{2,1,0:T(8,128)(2,1)} %broadcast_in_dim.32), calls=%async_computation | async-start | bytes 4194304 | tf_op jit(solution)/shard_map/all_to_all | solution.py:25
  48.8 3.1 copy-start.10
  96.1 173.7 %dynamic-slice-start = ((f32[2048]{0:T(1024)}, s32[]{:T(128)}), f32[1024]{0:T(1024)S(1)}, s32[]{:S(2)}) async-start(f32[2048]{0:T(1024)} %param.18, s32[]{:T(128)} %select_n.51), calls=%async_computation.10 | async-start | bytes 8704 | tf_op jit(solution)/shard_map/dynamic_slice | solution.py:121
  96.1 173.7 %dynamic-slice-start.1 = ((f32[2048]{0:T(1024)}, s32[]{:T(128)}), f32[1024]{0:T(1024)S(1)}, s32[]{:S(2)}) async-start(f32[2048]{0:T(1024)} %param.19, s32[]{:T(128)} %select_n.51), calls=%async_computation.11 | async-start | bytes 8704 | tf_op jit(solution)/shard_map/dynamic_slice | solution.py:122
  282.3 5.4 %copy-start.2 = (bf16[2,4,4,1024,64]{3,4,2,1,0:T(8,128)(2,1)S(1)}, bf16[2,4,4,1024,64]{3,4,2,1,0:T(8,128)(2,1)}, u32[]{:S(2)}) copy-start(bf16[2,4,4,1024,64]{3,4,2,1,0:T(8,128)(2,1)} %copy.57) | copy-start | bytes 12582916
  296.8 5.6 %copy-start.5 = (bf16[1408,64]{0,1:T(8,128)(2,1)S(1)}, bf16[1408,64]{0,1:T(8,128)(2,1)}, u32[]{:S(2)}) copy-start(bf16[1408,64]{0,1:T(8,128)(2,1)} %param.27) | copy-start | bytes 540676
  305.5 192.9 %all-to-all-start.4 = ((bf16[32,1408,64]{1,2,0:T(8,128)(2,1)}), bf16[32,1408,64]{1,2,0:T(8,128)(2,1)}, u32[]{:S(2)}, u32[]{:S(2)}) async-start(bf16[32,1408,64]{1,2,0:T(8,128)(2,1)} %stack.2), calls=%async_computation.4 | async-start | bytes 11534336 | tf_op jit(solution)/shard_map/all_to_all | solution.py:158
  312.9 1.5 copy-start.11
  482.3 10.4 %slice-start = ((s8[11534336]{0:T(1024)(128)(4,1)}), s8[4194304]{0:T(1024)(128)(4,1)S(1)}, s32[]{:S(2)}) async-start(s8[11534336]{0:T(1024)(128)(4,1)} %bitcast.60), calls=%async_computation.12 | async-start | bytes 8388608
  482.3 10.4 %slice-start.1 = ((s8[11534336]{0:T(1024)(128)(4,1)}), s8[4194304]{0:T(1024)(128)(4,1)S(1)}, s32[]{:S(2)}) async-start(s8[11534336]{0:T(1024)(128)(4,1)} %bitcast.60), calls=%async_computation.13 | async-start | bytes 8388608
  489.1 3.6 slice-start.2
  490.9 3.0 copy-start.4
  528.4 1.8 copy-start.1
Sparse Core Ops, SparseCore 0:
  14.2 24.7 all-gather.7
  40.6 50.3 all-gather.9
  92.7 146.3 all-gather.5
  240.7 241.5 all-gather.11
